TPU v7x, 32 devices: a whole 2x2x4 slice. The times are simulated.
32 devices in a mesh: fs: 4 (over y, x), tp: 8 (over z, core).
Axes of the slice: x: 2, y: 2, z: 4, core: 2. Of those that a mesh axis runs over, the one named last changes fastest.
Arguments:
- prompt: bfloat16 [4096, 2048], P(('fs', 'tp')), may hold values from -6 to 6
- norm_gain: float32 [2048], P('tp'), may hold values from 0.1 to 1.9
- gate_master: float32 [8, 2, 512, 2048], P(None, None, 'fs', 'tp'), may hold values from -0.125 to 0.125
- up_master: float32 [8, 2, 512, 2048], P(None, None, 'fs', 'tp'), may hold values from -0.125 to 0.125
- down_master: float32 [8, 2, 512, 2048], P(None, None, 'fs', 'tp'), may hold values from -0.25 to 0.25
- group_pick: int32 [4096, 1], P(('fs', 'tp')), may hold values from 0 to 7; in each aligned block of 128 rows (0 to 127, 128 to 255, ...) at most 32 rows name the same one
- route_weight: bfloat16 [4096, 2], P(('fs', 'tp')), may hold values from 0.099609375 to 1
Outputs:
- gate_serve: bfloat16 [8, 2, 512, 2048], P('tp', None, 'fs')
- up_serve: bfloat16 [8, 2, 512, 2048], P('tp', None, 'fs')
- down_serve: bfloat16 [8, 2, 512, 2048], P('tp', None, 'fs')
- mixed: bfloat16 [4096, 2048], P(('fs', 'tp'))
Inputs may be any that keep to these rules, and one draw needn't show every extreme that they name: `group_pick`: in the rows of one device no group is named by more than 32 rows, and in every draw some device's rows name one group exactly 32 times.
All inputs are finite; a program needn't handle non-finite values.
Results may differ from a plain program's by a relative error of at most 0.0081.
Values may be sent and summed in bfloat16 or wider, within the bound.
A program may use at most 64 MiB of HBM per device.

v0:
```python
import jax
import jax.numpy as jnp
from jax import lax
from jax.sharding import PartitionSpec as P

EPS = 1e-06


def expert_rows(group_rows, weights, pieces):
    gate_piece, up_piece, down_piece = pieces
    expert_count = gate_piece.shape[1]
    unit_count = gate_piece.shape[2]
    model_width = gate_piece.shape[3]
    row_count = group_rows.shape[0]
    gate_matrix = gate_piece.reshape(expert_count * unit_count, model_width)
    up_matrix = up_piece.reshape(expert_count * unit_count, model_width)
    down_matrix = down_piece.reshape(expert_count * unit_count, model_width)
    gate_pre = jnp.einsum("sd,hd->sh", group_rows, gate_matrix, preferred_element_type=jnp.float32)
    up_pre = jnp.einsum("sd,hd->sh", group_rows, up_matrix, preferred_element_type=jnp.float32)
    active = (jax.nn.silu(gate_pre) * up_pre).reshape(row_count, expert_count, unit_count)
    hidden = (weights.astype(jnp.float32)[:, :, None] * active).reshape(
        row_count, expert_count * unit_count
    )
    hidden = hidden.astype(jnp.bfloat16)
    return jnp.dot(hidden, down_matrix, preferred_element_type=jnp.float32)


def per_device(prompt, norm_gain, gate_master, up_master, down_master, group_pick, route_weight):
    group_total = lax.axis_size("tp")
    gate_local = (gate_master * norm_gain).astype(jnp.bfloat16)
    up_local = (up_master * norm_gain).astype(jnp.bfloat16)
    down_local = down_master.astype(jnp.bfloat16)
    gate_serve, up_serve, down_serve = (
        lax.all_to_all(gate_local, "tp", split_axis=0, concat_axis=3, tiled=True),
        lax.all_to_all(up_local, "tp", split_axis=0, concat_axis=3, tiled=True),
        lax.all_to_all(down_local, "tp", split_axis=0, concat_axis=3, tiled=True),
    )
    values = prompt.astype(jnp.float32)
    normed = (values * lax.rsqrt(jnp.mean(values * values, axis=1, keepdims=True) + EPS)).astype(
        jnp.bfloat16
    )
    tok_count = prompt.shape[0]
    capacity = 2 * tok_count // group_total
    slot_total = group_total * capacity
    chosen = group_pick[:, 0]
    member = (chosen[:, None] == jnp.arange(group_total, dtype=jnp.int32)[None, :]).astype(
        jnp.int32
    )
    slot_rank = jnp.sum(jnp.cumsum(member, axis=0) * member, axis=1) - 1
    target = chosen * capacity + slot_rank
    placing = (jnp.arange(slot_total, dtype=jnp.int32)[:, None] == target[None, :]).astype(
        jnp.bfloat16
    )
    send_rows = jnp.dot(placing, normed, preferred_element_type=jnp.float32).astype(jnp.bfloat16)
    send_weights = jnp.dot(placing, route_weight, preferred_element_type=jnp.float32).astype(
        jnp.bfloat16
    )
    got_rows, got_weights = (
        lax.all_to_all(
            send_rows.reshape(group_total, capacity, -1),
            "tp",
            split_axis=0,
            concat_axis=0,
            tiled=True,
        ),
        lax.all_to_all(
            send_weights.reshape(group_total, capacity, -1),
            "tp",
            split_axis=0,
            concat_axis=0,
            tiled=True,
        ),
    )
    group_rows = got_rows.reshape(slot_total, -1)
    weights = got_weights.reshape(slot_total, -1)
    gathered = (
        lax.all_gather(gate_serve, "fs", axis=2, tiled=True),
        lax.all_gather(up_serve, "fs", axis=2, tiled=True),
        lax.all_gather(down_serve, "fs", axis=2, tiled=True),
    )
    summed = expert_rows(group_rows, weights, gathered)
    result = summed.astype(jnp.bfloat16).reshape(group_total, capacity, -1)
    returned = lax.all_to_all(result, "tp", split_axis=0, concat_axis=0, tiled=True)
    mixed = jnp.einsum(
        "st,sd->td", placing, returned.reshape(slot_total, -1), preferred_element_type=jnp.float32
    ).astype(jnp.bfloat16)
    return (gate_serve, up_serve, down_serve, mixed)


def solution(mesh):
    placed = (
        P(("fs", "tp"), None),
        P("tp"),
        P(None, None, "fs", "tp"),
        P(None, None, "fs", "tp"),
        P(None, None, "fs", "tp"),
        P(("fs", "tp"), None),
        P(("fs", "tp"), None),
    )
    return jax.shard_map(
        per_device,
        mesh=mesh,
        in_specs=placed,
        out_specs=(
            P("tp", None, "fs", None),
            P("tp", None, "fs", None),
            P("tp", None, "fs", None),
            P(("fs", "tp"), None),
        ),
        check_vma=False,
    )
```

profile of v0, /device:TPU:0, one launch (start us, length us, event | category | flops | bytes accessed | tf_op | source)
XLA Modules:
  0.0 250.6 jit_solution(5716967491578532564)
XLA Ops:
  7.2 2.7 %multiply_convert_fusion = (bf16[8,2,128,256]{3,2,1,0:T(8,128)(2,1)S(1)}, bf16[8,2,128,256]{3,2,1,0:T(8,128)(2,1)S(1)}) fusion(f32[8,2,128,256]{3,2,1,0:T(8,128)} %param.10, f32[256]{0:T(256)} %param.8, f32[8,2,128,256]{3,2,1,0:T(8,128)} %param.9), kind=kLoop, calls=%fused_computation.3 | loop fusion | flops 2097152 | bytes 6292480 | tf_op jit(solution)/shard_map/convert_element_type | solution.py:31
  9.9 32.7 %all_to_all.69 = bf16[8,2,128,256]{3,2,1,0:T(8,128)(2,1)S(1)} all-to-all(bf16[8,2,128,256]{3,2,1,0:T(8,128)(2,1)S(1)} %get-tuple-element.5), channel_id=1, replica_groups=mesh['fs'=4,'tp'=8] {'tp'}, dimensions={0} | all-to-all | bytes 2097152 | tf_op jit(solution)/shard_map/all_to_all | solution.py:34
  42.7 1.1 copy.32
  43.8 29.0 %all_to_all.70 = bf16[8,2,128,256]{3,2,1,0:T(8,128)(2,1)S(1)} all-to-all(bf16[8,2,128,256]{3,2,1,0:T(8,128)(2,1)S(1)} %get-tuple-element.4), channel_id=1, replica_groups=mesh['fs'=4,'tp'=8] {'tp'}, dimensions={0} | all-to-all | bytes 2097152 | tf_op jit(solution)/shard_map/all_to_all | solution.py:35
  72.8 1.1 copy.33
  74.2 29.0 %all_to_all.71 = bf16[8,2,128,256]{3,2,1,0:T(8,128)(2,1)S(1)} all-to-all(bf16[8,2,128,256]{3,2,1,0:T(8,128)(2,1)S(1)} %convert_element_type.46), channel_id=1, replica_groups=mesh['fs'=4,'tp'=8] {'tp'}, dimensions={0} | all-to-all | bytes 2097152 | tf_op jit(solution)/shard_map/all_to_all | solution.py:36
  103.1 1.1 copy.34
  104.4 0.2 reduce_window_sum.11
  104.5 0.2 select_reduce_fusion
  105.0 0.6 copy.28
  105.6 3.3 %all-to-all-start.3 = ((bf16[8,32,2]{1,2,0:T(2,128)(2,1)}), bf16[8,32,2]{1,2,0:T(2,128)(2,1)S(1)}, u32[]{:S(2)}, u32[]{:S(2)}) async-start(bf16[8,32,2]{1,2,0:T(2,128)(2,1)} %copy.28), calls=%async_computation.3 | async-start | bytes 8192 | tf_op jit(solution)/shard_map/all_to_all | solution.py:66
  108.9 0.2 fusion.2
  109.1 1.6 convolution_convert_fusion
  110.7 3.7 %all-to-all-done.3 = bf16[8,32,2]{1,2,0:T(2,128)(2,1)S(1)} async-done(((bf16[8,32,2]{1,2,0:T(2,128)(2,1)}), bf16[8,32,2]{1,2,0:T(2,128)(2,1)S(1)}, u32[]{:S(2)}, u32[]{:S(2)}) %all-to-all-start.3) | async-done | bytes 1056 | tf_op jit(solution)/shard_map/all_to_all | solution.py:66
  114.3 3.6 %all-to-all-start.4 = ((bf16[8,32,2048]{2,1,0:T(8,128)(2,1)}), bf16[8,32,2048]{2,1,0:T(8,128)(2,1)S(1)}, u32[]{:S(2)}, u32[]{:S(2)}) async-start(bf16[8,32,2048]{2,1,0:T(8,128)(2,1)} %bitcast.8), calls=%async_computation.4 | async-start | bytes 2097152 | tf_op jit(solution)/shard_map/all_to_all | solution.py:59
  118.0 0.3 mul.62
  118.4 0.2 copy.35
  118.6 25.8 %all-to-all-done.4 = bf16[8,32,2048]{2,1,0:T(8,128)(2,1)S(1)} async-done(((bf16[8,32,2048]{2,1,0:T(8,128)(2,1)}), bf16[8,32,2048]{2,1,0:T(8,128)(2,1)S(1)}, u32[]{:S(2)}, u32[]{:S(2)}) %all-to-all-start.4) | async-done | bytes 1048608 | tf_op jit(solution)/shard_map/all_to_all | solution.py:59
  144.4 4.6 %fusion.12 = f32[256,1024]{1,0:T(8,128)} fusion(bf16[256,2048]{1,0:T(8,128)(2,1)S(1)} %bitcast.47, bf16[1024,2048]{1,0:T(8,128)(2,1)} %bitcast.54), kind=kOutput, calls=%fused_computation.26 | convolution fusion | flops 1073741824 | bytes 6291456 | tf_op jit(solution)/shard_map/sd,hd->sh/dot_general | solution.py:18
  149.0 1.4 all-gather.6.cloned.1.call-done
  150.5 55.0 %all-gather.8.cloned.1.call-done = bf16[1,2,512,2048]{3,2,1,0:T(8,128)(2,1)} async-done(((bf16[1,2,128,2048]{3,2,1,0:T(8,128)(2,1)}), bf16[1,2,512,2048]{3,2,1,0:T(8,128)(2,1)}) %all-gather.8.cloned.1.call-update) | async-done | bytes 4194320 | tf_op jit(solution)/shard_map/all_gather | solution.py:79
  205.5 6.4 %convolution_convert_fusion.1 = bf16[256,2048]{1,0:T(8,128)(2,1)S(1)} fusion(bf16[1024,2048]{1,0:T(8,128)(2,1)} %bitcast.56, f32[256,1024]{1,0:T(8,128)S(1)} %bitcast.49, bf16[256,2048]{1,0:T(8,128)(2,1)S(1)} %bitcast.48, bf16[1024,2048]{1,0:T(8,128)(2,1)} %bitcast.55, f32[256,1024]{1,0:T(8,128)} %fusion.12), kind=kOutput, calls=%fused_computation.1 | convolution fusion | flops 2149842944 | bytes 12582912 | tf_op jit(solution)/shard_map/dot_general | solution.py:25
  211.9 31.0 %all_to_all.72 = bf16[8,32,2048]{2,1,0:T(8,128)(2,1)S(1)} all-to-all(bf16[8,32,2048]{2,1,0:T(8,128)(2,1)S(1)} %bitcast.50), channel_id=1, replica_groups=mesh['fs'=4,'tp'=8] {'tp'}, dimensions={0} | all-to-all | bytes 2097152 | tf_op jit(solution)/shard_map/all_to_all | solution.py:83
  242.9 1.1 convolution_convert_fusion.2
  (23 shorter events, 0.8 us)
Async XLA Ops:
  7.2 97.6 %copy-start = (bf16[128,2]{0,1:T(2,128)(2,1)S(1)}, bf16[128,2]{0,1:T(2,128)(2,1)}, u32[]{:S(2)}) copy-start(bf16[128,2]{0,1:T(2,128)(2,1)} %param.13) | copy-start | bytes 1540
  7.2 137.2 %all-gather.4.cloned.1.call-start = ((), (), s32[]{:S(2)}) async-start(), calls=%async_computation.6 | async-start | bytes 5242880 | tf_op jit(solution)/shard_map/all_gather | solution.py:77
  42.7 31.4 %copy-start.1 = (f32[8,2,128,256]{3,2,1,0:T(8,128)S(1)}, f32[8,2,128,256]{3,2,1,0:T(8,128)}, u32[]{:S(2)}) copy-start(f32[8,2,128,256]{3,2,1,0:T(8,128)} %param.11) | copy-start | bytes 6291460
  43.8 106.7 %all-gather.6.cloned.1.call-start = ((), (), s32[]{:S(2)}) async-start(), calls=%async_computation.7 | async-start | bytes 5242880 | tf_op jit(solution)/shard_map/all_gather | solution.py:78
  73.9 30.3 %copy-start.3 = (s32[128,1]{0,1:T(1,128)S(1)}, s32[128,1]{0,1:T(1,128)}, u32[]{:S(2)}) copy-start(s32[128,1]{0,1:T(1,128)} %param.12) | copy-start | bytes 1540
  73.9 35.0 %copy-start.2 = (bf16[128,2048]{1,0:T(8,128)(2,1)S(1)}, bf16[128,2048]{1,0:T(8,128)(2,1)}, u32[]{:S(2)}) copy-start(bf16[128,2048]{1,0:T(8,128)(2,1)} %param.7) | copy-start | bytes 1572868
  74.0 131.5 %all-gather.8.cloned.1.call-start = ((), (), s32[]{:S(2)}) async-start(), calls=%async_computation.8 | async-start | bytes 5242880 | tf_op jit(solution)/shard_map/all_gather | solution.py:79
  105.6 8.8 %all-to-all-start.3 = ((bf16[8,32,2]{1,2,0:T(2,128)(2,1)}), bf16[8,32,2]{1,2,0:T(2,128)(2,1)S(1)}, u32[]{:S(2)}, u32[]{:S(2)}) async-start(bf16[8,32,2]{1,2,0:T(2,128)(2,1)} %copy.28), calls=%async_computation.3 | async-start | bytes 8192 | tf_op jit(solution)/shard_map/all_to_all | solution.py:66
  114.3 30.1 %all-to-all-start.4 = ((bf16[8,32,2048]{2,1,0:T(8,128)(2,1)}), bf16[8,32,2048]{2,1,0:T(8,128)(2,1)S(1)}, u32[]{:S(2)}, u32[]{:S(2)}) async-start(bf16[8,32,2048]{2,1,0:T(8,128)(2,1)} %bitcast.8), calls=%async_computation.4 | async-start | bytes 2097152 | tf_op jit(solution)/shard_map/all_to_all | solution.py:59
Sparse Core Ops, SparseCore 0:
  43.9 51.4 all-gather.3
  97.9 52.5 all-gather.5
  152.9 52.5 all-gather.7
where the time goes:
time: 251 us
  blocking collectives  122 us (49%)
  waiting for transfers between devices  86 us (34%)
  matrix products  13.9 us (6%)
  between operations  13.9 us (6%)
  starting transfers between devices  6.99 us (3%)
  local copies, waits for them, and re-layouts  4.69 us (2%)
  other arithmetic  3.46 us (1%)
    all_gather x1, waiting for transfers between devices, per_device(): lax.all_gather(down_serve, 'fs', axis=2, tiled=True)  55 us
    all_to_all x1, blocking collectives, per_device(): lax.all_to_all(gate_local, 'tp', split_axis=0, concat_axis=3, tiled=True)  32.7 us
    all_to_all x1, blocking collectives, per_device(): lax.all_to_all(result, 'tp', split_axis=0, concat_axis=0, tiled=True)  31 us
    all_to_all x1, blocking collectives, per_device(): lax.all_to_all(up_local, 'tp', split_axis=0, concat_axis=3, tiled=True)  29 us
    all_to_all x1, blocking collectives, per_device(): lax.all_to_all(down_local, 'tp', split_axis=0, concat_axis=3, tiled=True)  29 us
    all_to_all x1, waiting for transfers between devices, per_device(): lax.all_to_all(send_rows.reshape(group_total, capacity, -1), 'tp', split_...  25.8 us
    dot_general x1, matrix products, expert_rows(): return jnp.dot(hidden, down_matrix, preferred_element_type=jnp.float32)  6.42 us
  transfers between devices with their start and end apart: 5, of which 4 were waited for; matrix products, arithmetic and copies ran while one was open for 4% of the time, Pallas kernels for 0%

commit v1 on v0

--- a/solution.py
+++ b/solution.py
@@ -1,9 +1,15 @@
+import functools
+
 import jax
 import jax.numpy as jnp
 from jax import lax
+from jax.experimental import pallas as pl
+from jax.experimental.pallas import tpu as pltpu
 from jax.sharding import PartitionSpec as P
 
 EPS = 1e-06
+MESH = pl.DeviceIdType.MESH
+LANES = 128
 
 
 def expert_rows(group_rows, weights, pieces):
@@ -25,16 +31,200 @@
     return jnp.dot(hidden, down_matrix, preferred_element_type=jnp.float32)
 
 
+def flipped(index, mask, size):
+    total, bit = 0, 1
+    while bit < size:
+        digit = lax.rem(lax.div(index, bit), 2)
+        total = total + bit * ((1 - digit) if mask & bit else digit)
+        bit *= 2
+    return total
+
+
+def exchange_kernel(
+    dims,
+    gate_in, up_in, down_in, rows_in, placing_ref,
+    gate_out, up_out, down_out, mixed_ref,
+    xrows, hidden, psend, racc, rsum, ret,
+    rows_s, rows_r, w_s, w_r, fwd_s, fwd_r, red_s, red_r, ret_s, ret_r, loc,
+):
+    fs_n, tp_n, experts, units, width, model, cap = dims
+    f = lax.axis_index("fs")
+    t = lax.axis_index("tp")
+    tp_peer = [flipped(t, k, tp_n) for k in range(tp_n)]
+    fs_peer = [flipped(f, j, fs_n) for j in range(fs_n)]
+
+    barrier = pltpu.get_barrier_semaphore()
+    for k in range(1, tp_n):
+        pl.semaphore_signal(barrier, inc=1, device_id=(f, tp_peer[k]), device_id_type=MESH)
+    for j in range(1, fs_n):
+        pl.semaphore_signal(barrier, inc=1, device_id=(fs_peer[j], t), device_id_type=MESH)
+    pl.semaphore_wait(barrier, tp_n - 1 + fs_n - 1)
+
+    def columns(index):
+        return pl.ds(pl.multiple_of(index * width, width), width)
+
+    def remote(src, dst, send, recv, fs_to, tp_to):
+        return pltpu.make_async_remote_copy(
+            src_ref=src, dst_ref=dst, send_sem=send, recv_sem=recv,
+            device_id=(fs_to, tp_to), device_id_type=MESH,
+        )
+
+    far_first = list(range(tp_n - 1, 0, -1))
+    own_rows = pltpu.make_async_copy(rows_in.at[t], xrows.at[f, t], loc.at[0])
+    own_rows.start()
+    rows_copy = {}
+    for k in far_first:
+        rows_copy[k] = remote(
+            rows_in.at[tp_peer[k]], xrows.at[f, t], rows_s.at[k], rows_r.at[k], f, tp_peer[k]
+        )
+        rows_copy[k].start()
+    w_copy, own_w = {}, []
+    for m, (src, dst) in enumerate(((gate_in, gate_out), (up_in, up_out), (down_in, down_out))):
+        own = pltpu.make_async_copy(src.at[t], dst.at[:, columns(t)], loc.at[1 + m])
+        own.start()
+        own_w.append(own)
+        for k in far_first:
+            w_copy[m, k] = remote(
+                src.at[tp_peer[k]], dst.at[:, columns(t)], w_s.at[m, k], w_r.at[m, k], f, tp_peer[k]
+            )
+            w_copy[m, k].start()
+
+    fwd_copy = {}
+    for k in range(tp_n):
+        if k == 0:
+            own_rows.wait()
+        else:
+            rows_copy[k].wait_recv()
+        for j in range(fs_n - 1, 0, -1):
+            fwd_copy[k, j] = remote(
+                xrows.at[f, tp_peer[k]], xrows.at[f, tp_peer[k]],
+                fwd_s.at[k, j], fwd_r.at[k, j], fs_peer[j], t,
+            )
+            fwd_copy[k, j].start()
+    for copy in fwd_copy.values():
+        copy.wait_recv()
+    for m in range(2):
+        own_w[m].wait()
+        for k in range(1, tp_n):
+            w_copy[m, k].wait_recv()
+
+    block = tp_n * cap
+
+    @pl.loop(0, fs_n)
+    def _(b):
+        tile = xrows[b].reshape(block, model + LANES)
+        x = tile[:, :model]
+        route = tile[:, model:].astype(jnp.float32)
+        nt = (((1,), (1,)), ((), ()))
+        gate = lax.dot_general(x, gate_out[...], nt, preferred_element_type=jnp.float32)
+        up = lax.dot_general(x, up_out[...], nt, preferred_element_type=jnp.float32)
+        active = gate / (1.0 + jnp.exp(-gate)) * up
+        for e in range(experts):
+            at = slice(e * units, (e + 1) * units)
+            hidden[b, :, at] = (route[:, e : e + 1] * active[:, at]).astype(jnp.bfloat16)
+
+    red_copy = {}
+    ret_copy = {}
+
+    def reduce_and_return(k):
+        col = columns(tp_peer[k])
+        total = jnp.dot(hidden[f], down_out[:, col], preferred_element_type=jnp.float32)
+        for j in range(1, fs_n):
+            red_copy[k, j].wait_recv()
+            total = total + racc[k, j].astype(jnp.float32)
+        rsum[k] = total.astype(jnp.bfloat16).reshape(tp_n, cap, width)
+        for kk in far_first:
+            ret_copy[k, kk] = remote(
+                rsum.at[k, tp_peer[kk]], ret.at[t, :, col],
+                ret_s.at[k, kk], ret_r.at[k, kk], f, tp_peer[kk],
+            )
+            ret_copy[k, kk].start()
+        ret[t, :, col] = rsum[k, t]
+
+    for k in range(tp_n):
+        if k == 0:
+            own_w[2].wait()
+        else:
+            w_copy[2, k].wait_recv()
+        piece = down_out[:, columns(tp_peer[k])]
+        for j in range(fs_n - 1, 0, -1):
+            psend[k, j] = jnp.dot(
+                hidden[fs_peer[j]], piece, preferred_element_type=jnp.float32
+            ).astype(jnp.bfloat16)
+        for j in range(fs_n - 1, 0, -1):
+            red_copy[k, j] = remote(
+                psend.at[k, j], racc.at[k, j], red_s.at[k, j], red_r.at[k, j], fs_peer[j], t
+            )
+            red_copy[k, j].start()
+        if k >= 1:
+            reduce_and_return(k - 1)
+    reduce_and_return(tp_n - 1)
+
+    for copy in ret_copy.values():
+        copy.wait_recv()
+    mixed_ref[...] = lax.dot_general(
+        placing_ref[...], ret[...].reshape(block, model), (((0,), (0,)), ((), ())),
+        preferred_element_type=jnp.float32,
+    ).astype(jnp.bfloat16)
+
+    for group in (rows_copy, w_copy, fwd_copy, red_copy, ret_copy):
+        for copy in group.values():
+            copy.wait_send()
+
+
+def fused_device(fs_n, gate_local, up_local, down_local, normed, placing, route_weight, capacity):
+    tp_n, experts, units, width = gate_local.shape
+    tokens, model = normed.shape
+    packed = jnp.concatenate(
+        [normed, jnp.pad(route_weight, ((0, 0), (0, LANES - route_weight.shape[1])))], axis=1
+    )
+    rows = jnp.dot(placing, packed, preferred_element_type=jnp.float32).astype(jnp.bfloat16)
+    rows = rows.reshape(tp_n, capacity, model + LANES)
+    flat = experts * units
+    block = tp_n * capacity
+    bf16 = jnp.bfloat16
+    dma = pltpu.SemaphoreType.DMA
+    served = jax.ShapeDtypeStruct((flat, model), bf16)
+    vmem = pl.BlockSpec(memory_space=pltpu.VMEM)
+    hbm = pl.BlockSpec(memory_space=pl.ANY)
+    dims = (fs_n, tp_n, experts, units, width, model, capacity)
+    gate_serve, up_serve, down_serve, mixed = pl.pallas_call(
+        functools.partial(exchange_kernel, dims),
+        out_shape=(served, served, served, jax.ShapeDtypeStruct((tokens, model), bf16)),
+        in_specs=[hbm, hbm, hbm, hbm, vmem],
+        out_specs=(vmem, vmem, vmem, vmem),
+        scratch_shapes=[
+            pltpu.VMEM((fs_n, tp_n, capacity, model + LANES), bf16),
+            pltpu.VMEM((fs_n, block, flat), bf16),
+            pltpu.VMEM((tp_n, fs_n, block, width), bf16),
+            pltpu.VMEM((tp_n, fs_n, block, width), bf16),
+            pltpu.VMEM((tp_n, tp_n, capacity, width), bf16),
+            pltpu.VMEM((tp_n, capacity, model), bf16),
+            dma((tp_n,)), dma((tp_n,)),
+            dma((3, tp_n)), dma((3, tp_n)),
+            dma((tp_n, fs_n)), dma((tp_n, fs_n)),
+            dma((tp_n, fs_n)), dma((tp_n, fs_n)),
+            dma((tp_n, tp_n)), dma((tp_n, tp_n)),
+            dma((4,)),
+        ],
+        compiler_params=pltpu.CompilerParams(collective_id=0, has_side_effects=True),
+    )(
+        gate_local.reshape(tp_n, flat, width),
+        up_local.reshape(tp_n, flat, width),
+        down_local.reshape(tp_n, flat, width),
+        rows,
+        placing,
+    )
+    shape = (1, experts, units, model)
+    return gate_serve.reshape(shape), up_serve.reshape(shape), down_serve.reshape(shape), mixed
+
+
 def per_device(prompt, norm_gain, gate_master, up_master, down_master, group_pick, route_weight):
     group_total = lax.axis_size("tp")
+    fs_n = lax.axis_size("fs")
     gate_local = (gate_master * norm_gain).astype(jnp.bfloat16)
     up_local = (up_master * norm_gain).astype(jnp.bfloat16)
     down_local = down_master.astype(jnp.bfloat16)
-    gate_serve, up_serve, down_serve = (
-        lax.all_to_all(gate_local, "tp", split_axis=0, concat_axis=3, tiled=True),
-        lax.all_to_all(up_local, "tp", split_axis=0, concat_axis=3, tiled=True),
-        lax.all_to_all(down_local, "tp", split_axis=0, concat_axis=3, tiled=True),
-    )
     values = prompt.astype(jnp.float32)
     normed = (values * lax.rsqrt(jnp.mean(values * values, axis=1, keepdims=True) + EPS)).astype(
         jnp.bfloat16
@@ -50,6 +240,18 @@
     target = chosen * capacity + slot_rank
     placing = (jnp.arange(slot_total, dtype=jnp.int32)[:, None] == target[None, :]).astype(
         jnp.bfloat16
+    )
+    width, units = gate_master.shape[3], gate_master.shape[2]
+    small = group_total <= 8 and fs_n <= 4
+    even = (group_total & (group_total - 1)) == 0 and (fs_n & (fs_n - 1)) == 0
+    if small and even and width % LANES == 0 and units % LANES == 0 and capacity % 16 == 0:
+        return fused_device(
+            fs_n, gate_local, up_local, down_local, normed, placing, route_weight, capacity
+        )
+    gate_serve, up_serve, down_serve = (
+        lax.all_to_all(gate_local, "tp", split_axis=0, concat_axis=3, tiled=True),
+        lax.all_to_all(up_local, "tp", split_axis=0, concat_axis=3, tiled=True),
+        lax.all_to_all(down_local, "tp", split_axis=0, concat_axis=3, tiled=True),
     )
     send_rows = jnp.dot(placing, normed, preferred_element_type=jnp.float32).astype(jnp.bfloat16)
     send_weights = jnp.dot(placing, route_weight, preferred_element_type=jnp.float32).astype(

time: 251 us -> 165 us (0.66)
  Pallas kernels: 0 us -> 148 us
  blocking collectives: 122 us -> 0 us
  waiting for transfers between devices: 86 us -> 0 us
  between operations: 13.9 us -> 0.71 us
  matrix products: 13.9 us -> 1.43 us
  starting transfers between devices: 6.99 us -> 0 us
  other arithmetic: 3.46 us -> 8.54 us
    pallas_call x0 -> x1, Pallas kernels: none -> 148 us  [fused_device(): pl.pallas_call(functools.partial(exchange_kernel, dims), out_shape=(serve...]
    all_to_all x4 -> x0, blocking collectives: 122 us -> none  [the longest x1 32.7 us: per_device(): lax.all_to_all(gate_local, 'tp', split_axis=0, concat_axis=3, tiled=True)]
    all_gather x3 -> x0, waiting for transfers between devices: 56.5 us -> none  [the longest x1 55 us: per_device(): lax.all_gather(down_serve, 'fs', axis=2, tiled=True)]
    all_to_all x2 -> x0, waiting for transfers between devices: 29.5 us -> none  [the longest x1 25.8 us: per_device(): lax.all_to_all(send_rows.reshape(group_total, capacity, -1), 'tp', split_...]
    dot_general x5 -> x1, matrix products: 13.9 us -> 1.43 us  [fused_device(): jnp.dot(placing, packed, preferred_element_type=jnp.float32)]
    all_to_all x2 -> x0, starting transfers between devices: 6.87 us -> none  [the longest x1 3.56 us: per_device(): lax.all_to_all(send_rows.reshape(group_total, capacity, -1), 'tp', split_...]
    unnamed x9 -> x19, local copies, waits for them, and re-layouts: 0.22 us -> 6.21 us
    all_to_all x3 -> x0, local copies, waits for them, and re-layouts: 3.3 us -> none  [the longest x1 1.1 us: per_device(): lax.all_to_all(gate_local, 'tp', split_axis=0, concat_axis=3, tiled=True)]
  transfers between devices with their start and end apart: 5 -> 0, of which waited for: 4 -> 0; matrix products, arithmetic and copies ran while one was open for 4% -> 0% of each run, Pallas kernels for 0% -> 0%
where the time goes in v1:
time: 165 us
  Pallas kernels  148 us (90%)
  other arithmetic  8.54 us (5%)
  local copies, waits for them, and re-layouts  6.21 us (4%)
    pallas_call x1, Pallas kernels, fused_device(): pl.pallas_call(functools.partial(exchange_kernel, dims), out_shape=(serve...  148 us
    unnamed x19, local copies, waits for them, and re-layouts  6.21 us

profile of v1, /device:TPU:0, one launch (start us, length us, event | category | flops | bytes accessed | tf_op | source)
XLA Modules:
  0.0 164.7 jit_solution(7922705361476788799)
XLA Ops:
  0.6 0.0 copy-start
  0.6 1.4 fusion.1
  2.0 0.8 copy.12
  2.8 0.7 fusion.11
  3.6 0.2 reduce_window_sum.11
  3.7 0.8 select_reduce_fusion
  4.6 0.7 add_add_fusion
  5.2 0.7 fusion.9.placing_ref
  5.9 1.2 fusion.2
  7.1 0.0 copy-start.1
  7.1 0.0 copy-start.2
  7.1 0.0 copy-start.6
  7.1 1.4 convolution_convert_fusion
  8.5 0.0 copy-done
  8.6 1.1 convert_element_type.28
  9.7 0.2 copy-done.2
  9.9 1.8 %multiply_convert_fusion = (bf16[8,2,128,256]{3,2,1,0:T(8,128)(2,1)}, bf16[8,2,128,256]{3,2,1,0:T(8,128)(2,1)}) fusion(f32[8,2,128,256]{3,2,1,0:T(8,128)S(1)} %copy-done.1, f32[256]{0:T(256)S(1)} %copy-done.6, f32[8,2,128,256]{3,2,1,0:T(8,128)S(1)} %copy-done.2), kind=kLoop, calls=%fused_computation.1 | loop fusion | flops 2097152 | bytes 6292480 | tf_op jit(solution)/shard_map/convert_element_type | solution.py:226
  11.7 147.8 %shard_map.102 = (bf16[256,2048]{1,0:T(8,128)(2,1)}, bf16[256,2048]{1,0:T(8,128)(2,1)}, bf16[256,2048]{1,0:T(8,128)(2,1)}, bf16[128,2048]{1,0:T(8,128)(2,1)}) custom-call(bf16[8,256,256]{2,1,0:T(8,128)(2,1)} %bitcast.11, bf16[8,256,256]{2,1,0:T(8,128)(2,1)} %bitcast.10, bf16[8,256,256]{2,1,0:T(8,128)(2,1)} %bitcast.9, bf16[8,32,2176]{2,1,0:T(8,128)(2,1)} %bitcast.12, ...), custom_call_target="tpu_custom_call" | custom-call | tf_op jit(solution)/shard_map/pallas_call | solution.py:191
  159.5 0.0 copy-start.4
  159.5 0.0 copy-start.3
  159.5 2.5 %copy.17 = bf16[1,2,128,2048]{3,2,1,0:T(8,128)(2,1)} copy(bf16[1,2,128,2048]{3,2,1,0:T(8,128)(2,1)} %bitcast.15) | data formatting | bytes 2097152
  161.9 1.0 copy.18
  162.9 1.0 copy.19
  163.9 0.8 copy.20
  (7 shorter events, 0.0 us)
Async XLA Ops:
  0.6 7.9 %copy-start = (f32[8,2,128,256]{3,2,1,0:T(8,128)S(1)}, f32[8,2,128,256]{3,2,1,0:T(8,128)}, u32[]{:S(2)}) copy-start(f32[8,2,128,256]{3,2,1,0:T(8,128)} %param.11) | copy-start | bytes 6291460
  7.1 2.6 %copy-start.1 = (f32[8,2,128,256]{3,2,1,0:T(8,128)S(1)}, f32[8,2,128,256]{3,2,1,0:T(8,128)}, u32[]{:S(2)}) copy-start(f32[8,2,128,256]{3,2,1,0:T(8,128)} %param.10) | copy-start | bytes 6291460
  7.1 2.8 %copy-start.2 = (f32[8,2,128,256]{3,2,1,0:T(8,128)S(1)}, f32[8,2,128,256]{3,2,1,0:T(8,128)}, u32[]{:S(2)}) copy-start(f32[8,2,128,256]{3,2,1,0:T(8,128)} %param.9) | copy-start | bytes 6291460
  7.1 2.8 %copy-start.6 = (f32[256]{0:T(256)S(1)}, f32[256]{0:T(256)}, u32[]{:S(2)}) copy-start(f32[256]{0:T(256)} %param.8) | copy-start | bytes 3076
  159.5 2.5 %copy-start.4 = (bf16[256,2048]{1,0:T(8,128)(2,1)S(1)}, bf16[256,2048]{1,0:T(8,128)(2,1)}, u32[]{:S(2)}) copy-start(bf16[256,2048]{1,0:T(8,128)(2,1)} %get-tuple-element.9) | copy-start | bytes 3145732
  159.5 3.4 %copy-start.3 = (bf16[256,2048]{1,0:T(8,128)(2,1)S(1)}, bf16[256,2048]{1,0:T(8,128)(2,1)}, u32[]{:S(2)}) copy-start(bf16[256,2048]{1,0:T(8,128)(2,1)} %get-tuple-element.10) | copy-start | bytes 3145732
  161.9 1.9 %copy-start.5 = (bf16[128,2048]{1,0:T(8,128)(2,1)S(1)}, bf16[128,2048]{1,0:T(8,128)(2,1)}, u32[]{:S(2)}) copy-start(bf16[128,2048]{1,0:T(8,128)(2,1)} %get-tuple-element.21) | copy-start | bytes 1572868

commit v2 on v1

--- a/solution.py
+++ b/solution.py
@@ -44,8 +44,8 @@
     dims,
     gate_in, up_in, down_in, rows_in, placing_ref,
     gate_out, up_out, down_out, mixed_ref,
-    xrows, hidden, psend, racc, rsum, ret,
-    rows_s, rows_r, w_s, w_r, fwd_s, fwd_r, red_s, red_r, ret_s, ret_r, loc,
+    xrows, hidden, psend, racc, qsend, qacc, rsum, ret,
+    rows_s, rows_r, w_s, w_r, fwd_s, fwd_r, red_s, red_r, sec_s, sec_r, ret_s, ret_r, loc,
 ):
     fs_n, tp_n, experts, units, width, model, cap = dims
     f = lax.axis_index("fs")
@@ -69,7 +69,8 @@
             device_id=(fs_to, tp_to), device_id_type=MESH,
         )
 
-    far_first = list(range(tp_n - 1, 0, -1))
+    far_first = [1] + list(range(tp_n - 1, 1, -1))
+    pieces = [0] + far_first
     own_rows = pltpu.make_async_copy(rows_in.at[t], xrows.at[f, t], loc.at[0])
     own_rows.start()
     rows_copy = {}
@@ -87,13 +88,14 @@
             w_copy[m, k] = remote(
                 src.at[tp_peer[k]], dst.at[:, columns(t)], w_s.at[m, k], w_r.at[m, k], f, tp_peer[k]
             )
-            w_copy[m, k].start()
 
     fwd_copy = {}
-    for k in range(tp_n):
+    for k in pieces:
         if k == 0:
             own_rows.wait()
         else:
+            rows_copy[k].wait_send()
+            w_copy[0, k].start()
             rows_copy[k].wait_recv()
         for j in range(fs_n - 1, 0, -1):
             fwd_copy[k, j] = remote(
@@ -101,6 +103,10 @@
                 fwd_s.at[k, j], fwd_r.at[k, j], fs_peer[j], t,
             )
             fwd_copy[k, j].start()
+    for m in (1, 2):
+        for k in far_first:
+            w_copy[m - 1, k].wait_send()
+            w_copy[m, k].start()
     for copy in fwd_copy.values():
         copy.wait_recv()
     for m in range(2):
@@ -123,16 +129,44 @@
             at = slice(e * units, (e + 1) * units)
             hidden[b, :, at] = (route[:, e : e + 1] * active[:, at]).astype(jnp.bfloat16)
 
-    red_copy = {}
-    ret_copy = {}
+    first_copy, second_copy, ret_copy = {}, {}, {}
+    half = width // 2
+    order = ((1, 2), (2, 1))
+
+    def partial(index, k, h):
+        at = pl.ds(pl.multiple_of(tp_peer[k] * width + h * half, half), half)
+        return jnp.dot(hidden[index], down_out[:, at], preferred_element_type=jnp.float32)
+
+    def first_step(k):
+        for h, (a, b) in enumerate(order):
+            for n, index in enumerate((fs_peer[a], fs_peer[a ^ b])):
+                psend[k, h, n] = partial(index, k, h).astype(jnp.bfloat16)
+        for h, (a, b) in enumerate(order):
+            first_copy[k, h] = remote(
+                psend.at[k, h], racc.at[k, h], red_s.at[k, h], red_r.at[k, h], fs_peer[a], t
+            )
+            first_copy[k, h].start()
+
+    def second_step(k):
+        for h, (a, b) in enumerate(order):
+            part = partial(fs_peer[b], k, h)
+            first_copy[k, h].wait_recv()
+            qsend[k, h] = (part + racc[k, h, 1].astype(jnp.float32)).astype(jnp.bfloat16)
+        for h, (a, b) in enumerate(order):
+            second_copy[k, h] = remote(
+                qsend.at[k, h], qacc.at[k, h], sec_s.at[k, h], sec_r.at[k, h], fs_peer[b], t
+            )
+            second_copy[k, h].start()
 
     def reduce_and_return(k):
         col = columns(tp_peer[k])
-        total = jnp.dot(hidden[f], down_out[:, col], preferred_element_type=jnp.float32)
-        for j in range(1, fs_n):
-            red_copy[k, j].wait_recv()
-            total = total + racc[k, j].astype(jnp.float32)
-        rsum[k] = total.astype(jnp.bfloat16).reshape(tp_n, cap, width)
+        for h in range(2):
+            total = partial(f, k, h) + racc[k, h, 0].astype(jnp.float32)
+            second_copy[k, h].wait_recv()
+            total = total + qacc[k, h].astype(jnp.float32)
+            rsum[k, :, :, h * half : (h + 1) * half] = total.astype(jnp.bfloat16).reshape(
+                tp_n, cap, half
+            )
         for kk in far_first:
             ret_copy[k, kk] = remote(
                 rsum.at[k, tp_peer[kk]], ret.at[t, :, col],
@@ -141,24 +175,18 @@
             ret_copy[k, kk].start()
         ret[t, :, col] = rsum[k, t]
 
-    for k in range(tp_n):
-        if k == 0:
-            own_w[2].wait()
-        else:
-            w_copy[2, k].wait_recv()
-        piece = down_out[:, columns(tp_peer[k])]
-        for j in range(fs_n - 1, 0, -1):
-            psend[k, j] = jnp.dot(
-                hidden[fs_peer[j]], piece, preferred_element_type=jnp.float32
-            ).astype(jnp.bfloat16)
-        for j in range(fs_n - 1, 0, -1):
-            red_copy[k, j] = remote(
-                psend.at[k, j], racc.at[k, j], red_s.at[k, j], red_r.at[k, j], fs_peer[j], t
-            )
-            red_copy[k, j].start()
-        if k >= 1:
-            reduce_and_return(k - 1)
-    reduce_and_return(tp_n - 1)
+    for step in range(tp_n + 2):
+        if step < tp_n:
+            k = pieces[step]
+            if k == 0:
+                own_w[2].wait()
+            else:
+                w_copy[2, k].wait_recv()
+            first_step(k)
+        if 1 <= step <= tp_n:
+            second_step(pieces[step - 1])
+        if step >= 2:
+            reduce_and_return(pieces[step - 2])
 
     for copy in ret_copy.values():
         copy.wait_recv()
@@ -167,7 +195,9 @@
         preferred_element_type=jnp.float32,
     ).astype(jnp.bfloat16)
 
-    for group in (rows_copy, w_copy, fwd_copy, red_copy, ret_copy):
+    for k in far_first:
+        w_copy[2, k].wait_send()
+    for group in (fwd_copy, first_copy, second_copy, ret_copy):
         for copy in group.values():
             copy.wait_send()
 
@@ -196,14 +226,17 @@
         scratch_shapes=[
             pltpu.VMEM((fs_n, tp_n, capacity, model + LANES), bf16),
             pltpu.VMEM((fs_n, block, flat), bf16),
-            pltpu.VMEM((tp_n, fs_n, block, width), bf16),
-            pltpu.VMEM((tp_n, fs_n, block, width), bf16),
+            pltpu.VMEM((tp_n, 2, 2, block, width // 2), bf16),
+            pltpu.VMEM((tp_n, 2, 2, block, width // 2), bf16),
+            pltpu.VMEM((tp_n, 2, block, width // 2), bf16),
+            pltpu.VMEM((tp_n, 2, block, width // 2), bf16),
             pltpu.VMEM((tp_n, tp_n, capacity, width), bf16),
             pltpu.VMEM((tp_n, capacity, model), bf16),
             dma((tp_n,)), dma((tp_n,)),
             dma((3, tp_n)), dma((3, tp_n)),
             dma((tp_n, fs_n)), dma((tp_n, fs_n)),
-            dma((tp_n, fs_n)), dma((tp_n, fs_n)),
+            dma((tp_n, 2)), dma((tp_n, 2)),
+            dma((tp_n, 2)), dma((tp_n, 2)),
             dma((tp_n, tp_n)), dma((tp_n, tp_n)),
             dma((4,)),
         ],
@@ -242,9 +275,8 @@
         jnp.bfloat16
     )
     width, units = gate_master.shape[3], gate_master.shape[2]
-    small = group_total <= 8 and fs_n <= 4
-    even = (group_total & (group_total - 1)) == 0 and (fs_n & (fs_n - 1)) == 0
-    if small and even and width % LANES == 0 and units % LANES == 0 and capacity % 16 == 0:
+    small = group_total in (4, 8) and fs_n == 4
+    if small and width % (2 * LANES) == 0 and units % LANES == 0 and capacity % 16 == 0:
         return fused_device(
             fs_n, gate_local, up_local, down_local, normed, placing, route_weight, capacity
         )

time: 165 us -> 156 us (0.945)
  Pallas kernels: 148 us -> 139 us
    pallas_call x1, Pallas kernels: 148 us -> 139 us  [fused_device(): pl.pallas_call(functools.partial(exchange_kernel, dims), out_shape=(serve...]
where the time goes in v2:
time: 156 us
  Pallas kernels  139 us (89%)
  other arithmetic  8.54 us (5%)
  local copies, waits for them, and re-layouts  6.21 us (4%)
    pallas_call x1, Pallas kernels, fused_device(): pl.pallas_call(functools.partial(exchange_kernel, dims), out_shape=(serve...  139 us
    unnamed x19, local copies, waits for them, and re-layouts  6.21 us

profile of v2, /device:TPU:0, one launch (start us, length us, event | category | flops | bytes accessed | tf_op | source)
XLA Modules:
  0.0 156.1 jit_solution(10845844866042131391)
XLA Ops:
  0.6 0.0 copy-start
  0.6 1.4 fusion.1
  2.0 0.8 copy.12
  2.8 0.7 fusion.11
  3.6 0.2 reduce_window_sum.11
  3.7 0.8 select_reduce_fusion
  4.6 0.7 add_add_fusion
  5.2 0.7 fusion.9.placing_ref
  5.9 1.2 fusion.2
  7.1 0.0 copy-start.1
  7.1 0.0 copy-start.2
  7.1 0.0 copy-start.6
  7.1 1.4 convolution_convert_fusion
  8.6 1.1 convert_element_type.28
  9.7 0.2 copy-done.2
  9.9 1.8 %multiply_convert_fusion = (bf16[8,2,128,256]{3,2,1,0:T(8,128)(2,1)}, bf16[8,2,128,256]{3,2,1,0:T(8,128)(2,1)}) fusion(f32[8,2,128,256]{3,2,1,0:T(8,128)S(1)} %copy-done.1, f32[256]{0:T(256)S(1)} %copy-done.6, f32[8,2,128,256]{3,2,1,0:T(8,128)S(1)} %copy-done.2), kind=kLoop, calls=%fused_computation.1 | loop fusion | flops 2097152 | bytes 6292480 | tf_op jit(solution)/shard_map/convert_element_type | solution.py:259
  11.7 139.2 %shard_map.102 = (bf16[256,2048]{1,0:T(8,128)(2,1)}, bf16[256,2048]{1,0:T(8,128)(2,1)}, bf16[256,2048]{1,0:T(8,128)(2,1)}, bf16[128,2048]{1,0:T(8,128)(2,1)}) custom-call(bf16[8,256,256]{2,1,0:T(8,128)(2,1)} %bitcast.11, bf16[8,256,256]{2,1,0:T(8,128)(2,1)} %bitcast.10, bf16[8,256,256]{2,1,0:T(8,128)(2,1)} %bitcast.9, bf16[8,32,2176]{2,1,0:T(8,128)(2,1)} %bitcast.12, ...), custom_call_target="tpu_custom_call" | custom-call | tf_op jit(solution)/shard_map/pallas_call | solution.py:221
  150.9 2.5 %copy.17 = bf16[1,2,128,2048]{3,2,1,0:T(8,128)(2,1)} copy(bf16[1,2,128,2048]{3,2,1,0:T(8,128)(2,1)} %bitcast.15) | data formatting | bytes 2097152
  153.3 0.0 copy-done.4
  153.3 1.0 copy.18
  154.3 0.0 copy-done.3
  154.3 1.0 copy.19
  155.3 0.0 copy-done.5
  155.3 0.8 copy.20
  (7 shorter events, 0.0 us)
Async XLA Ops:
  0.6 7.9 %copy-start = (f32[8,2,128,256]{3,2,1,0:T(8,128)S(1)}, f32[8,2,128,256]{3,2,1,0:T(8,128)}, u32[]{:S(2)}) copy-start(f32[8,2,128,256]{3,2,1,0:T(8,128)} %param.11) | copy-start | bytes 6291460
  7.1 2.6 %copy-start.1 = (f32[8,2,128,256]{3,2,1,0:T(8,128)S(1)}, f32[8,2,128,256]{3,2,1,0:T(8,128)}, u32[]{:S(2)}) copy-start(f32[8,2,128,256]{3,2,1,0:T(8,128)} %param.10) | copy-start | bytes 6291460
  7.1 2.8 %copy-start.2 = (f32[8,2,128,256]{3,2,1,0:T(8,128)S(1)}, f32[8,2,128,256]{3,2,1,0:T(8,128)}, u32[]{:S(2)}) copy-start(f32[8,2,128,256]{3,2,1,0:T(8,128)} %param.9) | copy-start | bytes 6291460
  7.1 2.8 %copy-start.6 = (f32[256]{0:T(256)S(1)}, f32[256]{0:T(256)}, u32[]{:S(2)}) copy-start(f32[256]{0:T(256)} %param.8) | copy-start | bytes 3076
  150.9 2.5 %copy-start.4 = (bf16[256,2048]{1,0:T(8,128)(2,1)S(1)}, bf16[256,2048]{1,0:T(8,128)(2,1)}, u32[]{:S(2)}) copy-start(bf16[256,2048]{1,0:T(8,128)(2,1)} %get-tuple-element.9) | copy-start | bytes 3145732
  150.9 3.4 %copy-start.3 = (bf16[256,2048]{1,0:T(8,128)(2,1)S(1)}, bf16[256,2048]{1,0:T(8,128)(2,1)}, u32[]{:S(2)}) copy-start(bf16[256,2048]{1,0:T(8,128)(2,1)} %get-tuple-element.10) | copy-start | bytes 3145732
  153.3 1.9 %copy-start.5 = (bf16[128,2048]{1,0:T(8,128)(2,1)S(1)}, bf16[128,2048]{1,0:T(8,128)(2,1)}, u32[]{:S(2)}) copy-start(bf16[128,2048]{1,0:T(8,128)(2,1)} %get-tuple-element.21) | copy-start | bytes 1572868
